TPU v7x, 32 devices: a whole 2x2x4 slice. The times are simulated.
32 devices in a mesh: ep: 8 (over z, y), tp: 4 (over x, core).
Axes of the slice: x: 2, y: 2, z: 4, core: 2. Of those that a mesh axis runs over, the one named last changes fastest.
Arguments:
- tokens: bfloat16 [2048, 2048], P('ep', 'tp'), may hold values from -400 to 400
- expert_ids: int32 [2048, 2], P('ep'), may hold values from 0 to 7, all different within a row; in each aligned block of 256 rows (0 to 255, 256 to 511, ...) at most 80 rows name the same one
- route_weights: float32 [2048, 2], P('ep'), may hold values from 0.1 to 1
- pre_gain: float32 [2048], P('tp'), may hold values from 0.1 to 1.9
- post_gain: float32 [2048], P('tp'), may hold values from 0.1 to 1.9
- gate_weight: bfloat16 [8, 2048, 4096], P('ep', None, 'tp'), may hold values from -0.125 to 0.125
- up_weight: bfloat16 [8, 2048, 4096], P('ep', None, 'tp'), may hold values from -0.125 to 0.125
- down_weight: bfloat16 [8, 4096, 2048], P('ep', None, 'tp'), may hold values from -0.71875 to 0.71875
Outputs:
- layer_out: bfloat16 [2048, 2048], P('ep', 'tp')
Inputs may be any that keep to these rules, and one draw needn't show every extreme that they name: `expert_ids`: the 2 experts of a token are distinct. Within the rows of one device along ep, no expert is named more than 80 times, a bound that some block reaches.
All inputs are finite; a program needn't handle non-finite values.
Results may differ from a plain program's by a relative error of at most 0.007.
Values may be sent and summed in bfloat16 or wider, within the bound.
A program may use at most 64 MiB of HBM per device.

v0:
```python
import jax
import jax.numpy as jnp
from jax import lax
from jax.sharding import PartitionSpec as P

epsilon = 1e-06


def on_device(
    tokens, expert_ids, route_weights, pre_gain, post_gain, gate_weight, up_weight, down_weight
):
    tok_rows, width_part = tokens.shape
    width_full = width_part * lax.axis_size("tp")
    ep_count = lax.axis_size("ep")
    local_count = gate_weight.shape[0]
    experts_all = local_count * ep_count
    top_count = expert_ids.shape[1]
    capacity = max(2, tok_rows * top_count * 5 // (4 * experts_all))
    slot_total = experts_all * capacity
    tok_float = tokens.astype(jnp.float32)
    square_sum = lax.psum(jnp.sum(tok_float * tok_float, axis=1), "tp")
    inv_scale = lax.rsqrt(square_sum / width_full + epsilon)
    normed = (tok_float * inv_scale[:, None] * pre_gain[None, :]).astype(jnp.bfloat16)
    flat_ids = expert_ids.reshape(-1)
    onehot = (flat_ids[:, None] == jnp.arange(experts_all, dtype=jnp.int32)[None, :]).astype(
        jnp.int32
    )
    slot = jnp.sum((jnp.cumsum(onehot, axis=0) - 1) * onehot, axis=1)
    target = (flat_ids * capacity + slot).reshape(tok_rows, top_count)
    slot_index = jnp.arange(slot_total, dtype=jnp.int32)
    pick_map = (jnp.transpose(target).reshape(-1)[:, None] == slot_index[None, :]).astype(
        jnp.bfloat16
    )
    dispatch_map = jnp.sum(pick_map.reshape(top_count, tok_rows, slot_total), axis=0)
    outgoing = jnp.dot(
        jnp.transpose(dispatch_map), normed, preferred_element_type=jnp.float32
    ).astype(jnp.bfloat16)
    outgoing = outgoing.reshape(ep_count, local_count, capacity, width_part)
    arrived = lax.all_to_all(outgoing, "ep", split_axis=0, concat_axis=2, tiled=True)
    arrived = arrived.reshape(local_count, ep_count * capacity, width_part)
    row_total = ep_count * capacity
    features = lax.all_gather(arrived, "tp", axis=2, tiled=True)
    gate = jnp.einsum("erd,edh->erh", features, gate_weight, preferred_element_type=jnp.float32)
    upper = jnp.einsum("erd,edh->erh", features, up_weight, preferred_element_type=jnp.float32)
    hidden = (jax.nn.silu(gate) * upper).astype(jnp.bfloat16)
    hidden_whole = lax.all_gather(hidden, "tp", axis=2, tiled=True)
    result = jnp.einsum(
        "erh,ehd->erd", hidden_whole, down_weight, preferred_element_type=jnp.float32
    )
    expert_out = result.astype(jnp.bfloat16).reshape(1, local_count, row_total, width_part)
    returned = lax.all_to_all(expert_out, "ep", split_axis=2, concat_axis=0, tiled=True)
    returned = returned.reshape(slot_total, width_part)
    picked = jnp.dot(pick_map, returned, preferred_element_type=jnp.float32).reshape(
        top_count, tok_rows, width_part
    )
    mixed = jnp.sum(picked * jnp.transpose(route_weights)[:, :, None], axis=0)
    out_sum = lax.psum(jnp.sum(mixed * mixed, axis=1), "tp")
    out_scale = lax.rsqrt(out_sum / width_full + epsilon)
    return (mixed * out_scale[:, None] * post_gain[None, :]).astype(jnp.bfloat16)


def solution(mesh):
    return jax.shard_map(
        on_device,
        mesh=mesh,
        in_specs=(
            P("ep", "tp"),
            P("ep", None),
            P("ep", None),
            P("tp"),
            P("tp"),
            P("ep", None, "tp"),
            P("ep", None, "tp"),
            P("ep", None, "tp"),
        ),
        out_specs=P("ep", "tp"),
        check_vma=False,
    )
```

profile of v0, /device:TPU:0, one launch (start us, length us, event | category | flops | bytes accessed | tf_op | source)
XLA Modules:
  0.0 170.0 jit_solution(17323781832735627482)
XLA Ops:
  6.5 0.0 all-gather.4.cloned.1.call-start
  6.5 0.8 copy.39
  7.4 0.1 eq.65
  7.5 0.1 eq.61
  7.7 1.1 reduce-window.6
  8.8 0.2 slice_reduce_fusion
  9.1 0.1 fusion.34
  9.2 0.1 reduce_sum.51
  9.3 0.1 copy.41
  9.4 0.7 add_bitcast_fusion
  10.1 0.2 fusion.24
  10.3 1.1 fusion.28
  11.4 8.4 %psum.14 = f32[256]{0:T(256)S(1)} all-reduce(f32[256]{0:T(256)S(1)} %fusion.28), channel_id=1, replica_groups=mesh['ep'=8,'tp'=4] {'tp'}, use_global_device_ids=true, to_apply=%region_5.6 | all-reduce | flops 256 | bytes 2048 | tf_op jit(solution)/shard_map/psum | solution.py:21
  19.7 1.4 convolution_convert_fusion
  21.1 22.2 %all_to_all.8 = bf16[8,1,80,512]{3,2,1,0:T(8,128)(2,1)} all-to-all(bf16[8,1,80,512]{3,2,1,0:T(8,128)(2,1)S(1)} %bitcast.53), channel_id=1, replica_groups=mesh['ep'=8,'tp'=4] {'ep'}, dimensions={0} | all-to-all | bytes 1310720 | tf_op jit(solution)/shard_map/all_to_all | solution.py:39
  43.3 0.0 all-gather.4.cloned.1.call-update
  43.4 0.0 all-gather.6.cloned.1.call-start
  43.4 24.3 %all-gather.4.cloned.1.call-done = bf16[1,640,2048]{2,1,0:T(8,128)(2,1)} async-done(((bf16[1,640,512]{2,1,0:T(8,128)(2,1)}), bf16[1,640,2048]{2,1,0:T(8,128)(2,1)}) %all-gather.4.cloned.1.call-update) | async-done | bytes 2621456 | tf_op jit(solution)/shard_map/all_gather | solution.py:42
  67.8 0.0 copy-start.1
  67.8 0.0 copy-start.2
  67.8 5.6 %fusion.4 = f32[640,1024]{1,0:T(8,128)S(1)} fusion(bf16[1,2048,1024]{2,1,0:T(8,128)(2,1)} %param.13, bf16[1,640,2048]{2,1,0:T(8,128)(2,1)} %all-gather.4.cloned.1.call-done), kind=kOutput, calls=%fused_computation.4 | convolution fusion | flops 2684354560 | bytes 9437184 | tf_op jit(solution)/shard_map/erd,edh->erh/dot_general | solution.py:43
  73.4 0.0 copy-done.1
  73.4 0.0 copy-done.2
  73.4 4.2 %multiply_convert_fusion = bf16[640,1024]{1,0:T(8,128)(2,1)} fusion(f32[640,1024]{1,0:T(8,128)S(1)} %fusion.4, bf16[1,2048,1024]{2,1,0:T(8,128)(2,1)S(1)} %copy-done.1, bf16[1,640,2048]{2,1,0:T(8,128)(2,1)S(1)} %copy-done.2), kind=kOutput, calls=%fused_computation.8 | convolution fusion | flops 2688286720 | bytes 10747904 | tf_op jit(solution)/shard_map/erd,edh->erh/dot_general | solution.py:44
  77.6 0.0 all-gather.6.cloned.1.call-update
  77.6 40.6 %all-gather.6.cloned.1.call-done = bf16[640,4096]{1,0:T(8,128)(2,1)} async-done(((bf16[640,1024]{1,0:T(8,128)(2,1)}), bf16[640,4096]{1,0:T(8,128)(2,1)}) %all-gather.6.cloned.1.call-update) | async-done | bytes 5242896 | tf_op jit(solution)/shard_map/all_gather | solution.py:46
  118.2 6.6 %fusion.21 = bf16[1,1,640,512]{3,2,1,0:T(8,128)(2,1)S(1)} fusion(bf16[640,4096]{1,0:T(8,128)(2,1)} %all-gather.6.cloned.1.call-done, bf16[1,4096,512]{2,1,0:T(8,128)(2,1)} %param.15), kind=kOutput, calls=%fused_computation.17 | convolution fusion | flops 2684682240 | bytes 10092544 | tf_op jit(solution)/shard_map/erh,ehd->erd/dot_general | solution.py:47
  124.8 1.0 copy.50
  125.8 0.5 broadcast.77
  126.3 4.8 %reduce.3 = bf16[640,512]{1,0:T(8,128)(2,1)S(1)} reduce(bf16[640,1,1,512]{3,2,1,0:T(2,128)(2,1)S(1)} %bitcast.51, bf16[]{:T(256)} %broadcast.77), dimensions={1,2}, to_apply=%bitcast.50.reduce_sub_computation | reduce | bytes 1310722
  131.1 0.0 copy-start.3
  131.1 0.5 reshape.125
  131.6 23.4 %all_to_all.9 = bf16[8,2,20480]{2,1,0:T(2,128)(2,1)S(1)} all-to-all(bf16[8,2,20480]{2,1,0:T(2,128)(2,1)S(1)} %reshape.125), channel_id=1, replica_groups=mesh['ep'=8,'tp'=4] {'ep'}, dimensions={0} | all-to-all | bytes 1310720 | tf_op jit(solution)/shard_map/all_to_all | solution.py:51
  155.0 0.0 copy-start
  155.0 0.6 reshape.126
  155.6 0.0 copy-done.3
  155.6 0.6 fusion.18
  156.3 0.1 multiply_reduce_fusion
  156.4 6.0 %psum.15 = f32[256]{0:T(256)S(1)} all-reduce(f32[256]{0:T(256)S(1)} %multiply_reduce_fusion), channel_id=1, replica_groups=mesh['ep'=8,'tp'=4] {'tp'}, use_global_device_ids=true, to_apply=%region_8.9 | all-reduce | flops 256 | bytes 2048 | tf_op jit(solution)/shard_map/psum | solution.py:57
  162.4 0.0 copy-done
  162.4 0.8 multiply_convert_fusion.1
  (5 shorter events, 0.1 us)
Async XLA Ops:
  6.5 61.2 %all-gather.4.cloned.1.call-start = ((), (), s32[]{:S(2)}) async-start(), calls=%async_computation.2 | async-start | bytes 3276800 | tf_op jit(solution)/shard_map/all_gather | solution.py:42
  43.4 74.8 %all-gather.6.cloned.1.call-start = ((), (), s32[]{:S(2)}) async-start(), calls=%async_computation.3 | async-start | bytes 6553600 | tf_op jit(solution)/shard_map/all_gather | solution.py:46
  67.8 5.6 %copy-start.1 = (bf16[1,2048,1024]{2,1,0:T(8,128)(2,1)S(1)}, bf16[1,2048,1024]{2,1,0:T(8,128)(2,1)}, u32[]{:S(2)}) copy-start(bf16[1,2048,1024]{2,1,0:T(8,128)(2,1)} %param.14) | copy-start | bytes 12582916
  67.8 5.6 %copy-start.2 = (bf16[1,640,2048]{2,1,0:T(8,128)(2,1)S(1)}, bf16[1,640,2048]{2,1,0:T(8,128)(2,1)}, u32[]{:S(2)}) copy-start(bf16[1,640,2048]{2,1,0:T(8,128)(2,1)} %all-gather.4.cloned.1.call-done) | copy-start | bytes 7864324
  131.1 24.5 %copy-start.3 = (f32[256,2]{0,1:T(2,128)S(1)}, f32[256,2]{0,1:T(2,128)}, u32[]{:S(2)}) copy-start(f32[256,2]{0,1:T(2,128)} %param.10) | copy-start | bytes 6148
  155.0 7.4 %copy-start = (f32[512]{0:T(512)S(1)}, f32[512]{0:T(512)}, u32[]{:S(2)}) copy-start(f32[512]{0:T(512)} %param.12) | copy-start | bytes 6148
Sparse Core Ops, SparseCore 0:
  43.5 24.2 all-gather.3
  77.7 40.3 all-gather.5
where the time goes:
time: 170 us
  waiting for transfers between devices  64.9 us (38%)
  blocking collectives  59.9 us (35%)
  matrix products  18.4 us (11%)
  between operations  13.5 us (8%)
  other arithmetic  8.99 us (5%)
  local copies, waits for them, and re-layouts  4.19 us (2%)
    all_gather x1, waiting for transfers between devices, on_device(): hidden_whole = lax.all_gather(hidden, 'tp', axis=2, tiled=True)  40.6 us
    all_gather x1, waiting for transfers between devices, on_device(): features = lax.all_gather(arrived, 'tp', axis=2, tiled=True)  24.3 us
    all_to_all x1, blocking collectives, on_device(): lax.all_to_all(expert_out, 'ep', split_axis=2, concat_axis=0, tiled=True)  23.4 us
    all_to_all x1, blocking collectives, on_device(): lax.all_to_all(outgoing, 'ep', split_axis=0, concat_axis=2, tiled=True)  22.2 us
    psum x1, blocking collectives, on_device(): square_sum = lax.psum(jnp.sum(tok_float * tok_float, axis=1), 'tp')  8.37 us
    dot_general x1, matrix products, on_device(): jnp.einsum('erh,ehd->erd', hidden_whole, down_weight, preferred_element_t...  6.62 us
    psum x1, blocking collectives, on_device(): out_sum = lax.psum(jnp.sum(mixed * mixed, axis=1), 'tp')  5.95 us
    dot_general x1, matrix products, on_device(): jnp.einsum('erd,edh->erh', features, gate_weight, preferred_element_type=...  5.58 us
  transfers between devices with their start and end apart: 2, of which 2 were waited for; matrix products, arithmetic and copies ran while one was open for 0% of the time, Pallas kernels for 0%

commit v1 on v0

--- a/solution.py
+++ b/solution.py
@@ -9,6 +9,30 @@
 def on_device(
     tokens, expert_ids, route_weights, pre_gain, post_gain, gate_weight, up_weight, down_weight
 ):
+
+    def map_the_cube(z_in, axis_name, frame_in):
+        val = lax.axis_size(axis_name)
+        r1 = lax.axis_index(axis_name)
+        carry_out, far_arr, x_now = (val, r1, z_in.shape[2])
+        last = range(carry_out)
+        piece_next = map(lambda i0: (i0, (i0 + 1) % carry_out), last)
+        block_list = list(piece_next)
+        kept_arr = range(carry_out)
+        res = map(lambda i0: (i0, (i0 - 1) % carry_out), kept_arr)
+        pool = list(res)
+        right_arr = carry_out // 2
+        now = t_next = z_in
+        prior = frame_in(z_in, far_arr * x_now)
+        for u in [*range(1, right_arr + 1)]:
+            now = lax.ppermute(now, axis_name=axis_name, perm=block_list)
+            if u < carry_out - right_arr:
+                t_next = lax.ppermute(t_next, axis_name=axis_name, perm=pool)
+                n_now = frame_in(t_next, (far_arr + u) % carry_out * x_now)
+                prior = prior + n_now
+            tall = frame_in(now, (far_arr - u) % carry_out * x_now)
+            prior = prior + tall
+        return prior
+
     tok_rows, width_part = tokens.shape
     width_full = width_part * lax.axis_size("tp")
     ep_count = lax.axis_size("ep")
@@ -43,9 +67,15 @@
     gate = jnp.einsum("erd,edh->erh", features, gate_weight, preferred_element_type=jnp.float32)
     upper = jnp.einsum("erd,edh->erh", features, up_weight, preferred_element_type=jnp.float32)
     hidden = (jax.nn.silu(gate) * upper).astype(jnp.bfloat16)
-    hidden_whole = lax.all_gather(hidden, "tp", axis=2, tiled=True)
-    result = jnp.einsum(
-        "erh,ehd->erd", hidden_whole, down_weight, preferred_element_type=jnp.float32
+    result = map_the_cube(
+        hidden,
+        "tp",
+        lambda shard, offset: jnp.einsum(
+            "erh,ehd->erd",
+            shard,
+            lax.dynamic_slice_in_dim(down_weight, offset, shard.shape[2], axis=1),
+            preferred_element_type=jnp.float32,
+        ),
     )
     expert_out = result.astype(jnp.bfloat16).reshape(1, local_count, row_total, width_part)
     returned = lax.all_to_all(expert_out, "ep", split_axis=2, concat_axis=0, tiled=True)

time: 170 us -> 168 us (0.988)
  blocking collectives: 59.9 us -> 56.6 us
  starting transfers between devices: 0.04 us -> 1.8 us
    all_gather x1 -> x0, waiting for transfers between devices: 40.6 us -> none  [on_device(): hidden_whole = lax.all_gather(hidden, 'tp', axis=2, tiled=True)]
    ppermute x0 -> x3, waiting for transfers between devices: none -> 40.3 us  [the longest x2 40.3 us: map_the_cube(): now = lax.ppermute(now, axis_name=axis_name, perm=block_list)]
    all_to_all x1, blocking collectives: 23.4 us -> 20.1 us  [on_device(): lax.all_to_all(expert_out, 'ep', split_axis=2, concat_axis=0, tiled=True)]
    ppermute x0 -> x3, starting transfers between devices: none -> 1.8 us  [the longest x1 1.51 us: map_the_cube(): t_next = lax.ppermute(t_next, axis_name=axis_name, perm=pool)]
    dot_general x1 -> x4, matrix products: 6.62 us -> 7.39 us  [on_device(): jnp.einsum('erh,ehd->erd', shard, lax.dynamic_slice_in_dim(down_weight, o...]
  transfers between devices with their start and end apart: 2 -> 4, of which waited for: 2 -> 3; matrix products, arithmetic and copies ran while one was open for 0% -> 3% of each run, Pallas kernels for 0% -> 0%
where the time goes in v1:
time: 168 us; the launch traced here: 167 us
  waiting for transfers between devices  64.7 us (39%)
  blocking collectives  56.6 us (34%)
  matrix products  17.1 us (10%)
  between operations  13.5 us (8%)
  other arithmetic  8.99 us (5%)
  local copies, waits for them, and re-layouts  4.54 us (3%)
  starting transfers between devices  1.8 us (1%)
    ppermute x2, waiting for transfers between devices, map_the_cube(): now = lax.ppermute(now, axis_name=axis_name, perm=block_list)  40.3 us
    all_gather x1, waiting for transfers between devices, on_device(): features = lax.all_gather(arrived, 'tp', axis=2, tiled=True)  24.4 us
    all_to_all x1, blocking collectives, on_device(): lax.all_to_all(outgoing, 'ep', split_axis=0, concat_axis=2, tiled=True)  22.2 us
    all_to_all x1, blocking collectives, on_device(): lax.all_to_all(expert_out, 'ep', split_axis=2, concat_axis=0, tiled=True)  20.1 us
    psum x1, blocking collectives, on_device(): square_sum = lax.psum(jnp.sum(tok_float * tok_float, axis=1), 'tp')  8.37 us
    dot_general x4, matrix products, on_device(): jnp.einsum('erh,ehd->erd', shard, lax.dynamic_slice_in_dim(down_weight, o...  7.39 us
    psum x1, blocking collectives, on_device(): out_sum = lax.psum(jnp.sum(mixed * mixed, axis=1), 'tp')  5.94 us
    dot_general x1, matrix products, on_device(): jnp.einsum('erd,edh->erh', features, gate_weight, preferred_element_type=...  5.58 us
  transfers between devices with their start and end apart: 4, of which 3 were waited for; matrix products, arithmetic and copies ran while one was open for 3% of the time, Pallas kernels for 0%

profile of v1, /device:TPU:0, one launch (start us, length us, event | category | flops | bytes accessed | tf_op | source)
XLA Modules:
  0.0 167.3 jit_solution(6720261649194700914)
XLA Ops:
  6.5 0.0 copy-start
  6.5 0.0 copy-start.1
  6.5 0.0 all-gather.2.cloned.1.call-start
  6.5 0.8 copy.39
  7.4 0.1 eq.69
  7.5 0.1 eq.65
  7.7 1.1 reduce-window.6
  8.8 0.2 slice_reduce_fusion
  9.1 0.1 fusion.42
  9.2 0.1 reduce_sum.51
  9.4 0.1 copy.41
  9.4 0.7 add_bitcast_fusion
  10.1 0.2 fusion.32
  10.3 1.1 fusion.36
  11.4 8.4 %psum.14 = f32[256]{0:T(256)S(1)} all-reduce(f32[256]{0:T(256)S(1)} %fusion.36), channel_id=1, replica_groups=mesh['ep'=8,'tp'=4] {'tp'}, use_global_device_ids=true, to_apply=%region_5.6 | all-reduce | flops 256 | bytes 2048 | tf_op jit(solution)/shard_map/psum | solution.py:45
  19.8 0.0 copy-done
  19.8 0.0 copy-done.1
  19.8 0.4 convolution_convert_fusion
  20.2 22.2 %all_to_all.8 = bf16[8,1,80,512]{3,2,1,0:T(8,128)(2,1)} all-to-all(bf16[8,1,80,512]{3,2,1,0:T(8,128)(2,1)S(1)} %bitcast.70), channel_id=1, replica_groups=mesh['ep'=8,'tp'=4] {'ep'}, dimensions={0} | all-to-all | bytes 1310720 | tf_op jit(solution)/shard_map/all_to_all | solution.py:63
  42.4 0.0 all-gather.2.cloned.1.call-update
  42.5 24.4 %all-gather.2.cloned.1.call-done = bf16[1,640,2048]{2,1,0:T(8,128)(2,1)} async-done(((bf16[1,640,512]{2,1,0:T(8,128)(2,1)}), bf16[1,640,2048]{2,1,0:T(8,128)(2,1)}) %all-gather.2.cloned.1.call-update) | async-done | bytes 2621456 | tf_op jit(solution)/shard_map/all_gather | solution.py:66
  66.9 0.0 copy-start.3
  66.9 0.0 copy-start.5
  66.9 5.6 %fusion.2 = f32[640,1024]{1,0:T(8,128)S(1)} fusion(bf16[1,2048,1024]{2,1,0:T(8,128)(2,1)} %param.13, bf16[1,640,2048]{2,1,0:T(8,128)(2,1)} %all-gather.2.cloned.1.call-done), kind=kOutput, calls=%fused_computation.2 | convolution fusion | flops 2684354560 | bytes 9437184 | tf_op jit(solution)/shard_map/erd,edh->erh/dot_general | solution.py:67
  72.5 0.0 copy-done.3
  72.5 0.0 copy-done.5
  72.5 3.1 %multiply_convert_fusion = bf16[640,1024]{1,0:T(8,128)(2,1)S(1)} fusion(f32[640,1024]{1,0:T(8,128)S(1)} %fusion.2, bf16[1,2048,1024]{2,1,0:T(8,128)(2,1)S(1)} %copy-done.3, bf16[1,640,2048]{2,1,0:T(8,128)(2,1)S(1)} %copy-done.5), kind=kOutput, calls=%fused_computation.6 | convolution fusion | flops 2688286720 | bytes 10747904 | tf_op jit(solution)/shard_map/erd,edh->erh/dot_general | solution.py:68
  75.6 0.3 collective-permute-start.1
  75.9 1.5 collective-permute-start
  77.4 28.7 %collective-permute-done.1 = bf16[1,640,1024]{2,1,0:T(8,128)(2,1)S(1)} collective-permute-done((bf16[1,640,1024]{2,1,0:T(8,128)(2,1)S(1)}, bf16[1,640,1024]{2,1,0:T(8,128)(2,1)S(1)}, u32[]{:S(2)}, u32[]{:S(2)}) %collective-permute-start.1) | collective-permute-done | bytes 1310752 | tf_op jit(solution)/shard_map/ppermute | solution.py:27
  106.1 0.0 collective-permute-start.2
  106.1 0.0 copy-start.4
  106.1 2.2 %fusion.26 = f32[640,512]{1,0:T(8,128)S(1)} fusion(bf16[640,1024]{1,0:T(8,128)(2,1)S(1)} %multiply_convert_fusion, bf16[1,4096,512]{2,1,0:T(8,128)(2,1)} %param.15, s32[]{:T(128)S(6)} %select_n.27), kind=kOutput, calls=%fused_computation.25 | convolution fusion | flops 671088640 | bytes 3670020 | tf_op jit(solution)/shard_map/erh,ehd->erd/dot_general | solution.py:73
  108.3 0.0 collective-permute-done
  108.3 0.3 copy-done.4
  108.6 2.2 %convolution_add_fusion.2 = f32[640,512]{1,0:T(8,128)S(1)} fusion(f32[640,512]{1,0:T(8,128)S(1)} %fusion.26, bf16[1,640,1024]{2,1,0:T(8,128)(2,1)} %collective-permute-done, bf16[1,4096,512]{2,1,0:T(8,128)(2,1)S(1)} %copy-done.4, s32[]{:T(128)S(6)} %select_n.29), kind=kOutput, calls=%fused_computation.9 | convolution fusion | flops 671416320 | bytes 4980740 | tf_op jit(solution)/shard_map/erh,ehd->erd/dot_general | solution.py:73
  110.7 0.9 convolution_add_fusion.1
  111.6 11.6 %collective-permute-done.2 = bf16[1,640,1024]{2,1,0:T(8,128)(2,1)} collective-permute-done((bf16[1,640,1024]{2,1,0:T(8,128)(2,1)S(1)}, bf16[1,640,1024]{2,1,0:T(8,128)(2,1)}, u32[]{:S(2)}, u32[]{:S(2)}) %collective-permute-start.2) | collective-permute-done | bytes 1310752 | tf_op jit(solution)/shard_map/ppermute | solution.py:27
  123.2 2.2 %fusion.20 = bf16[1,1,640,512]{3,2,1,0:T(8,128)(2,1)S(1)} fusion(f32[640,512]{1,0:T(8,128)S(1)} %convolution_add_fusion.1, bf16[1,640,1024]{2,1,0:T(8,128)(2,1)} %collective-permute-done.2, bf16[1,4096,512]{2,1,0:T(8,128)(2,1)S(1)} %copy-done.4, s32[]{:T(128)S(6)} %select_n.33), kind=kOutput, calls=%fused_computation.21 | convolution fusion | flops 671744000 | bytes 4325380 | tf_op jit(solution)/shard_map/erh,ehd->erd/dot_general | solution.py:73
  125.4 1.0 copy.50
  126.4 0.5 broadcast.80
  126.9 4.8 %reduce.3 = bf16[640,512]{1,0:T(8,128)(2,1)S(1)} reduce(bf16[640,1,1,512]{3,2,1,0:T(2,128)(2,1)S(1)} %bitcast.68, bf16[]{:T(256)} %broadcast.80), dimensions={1,2}, to_apply=%bitcast.67.reduce_sub_computation | reduce | bytes 1310722
  131.7 0.5 reshape.151
  132.2 20.1 %all_to_all.9 = bf16[8,2,20480]{2,1,0:T(2,128)(2,1)S(1)} all-to-all(bf16[8,2,20480]{2,1,0:T(2,128)(2,1)S(1)} %reshape.151), channel_id=1, replica_groups=mesh['ep'=8,'tp'=4] {'ep'}, dimensions={0} | all-to-all | bytes 1310720 | tf_op jit(solution)/shard_map/all_to_all | solution.py:81
  152.3 0.0 copy-start.6
  152.3 0.6 reshape.152
  152.9 0.0 copy-done.6
  153.0 0.0 copy-start.2
  153.0 0.6 fusion.17
  153.6 0.1 multiply_reduce_fusion
  153.7 5.9 %psum.15 = f32[256]{0:T(256)S(1)} all-reduce(f32[256]{0:T(256)S(1)} %multiply_reduce_fusion), channel_id=1, replica_groups=mesh['ep'=8,'tp'=4] {'tp'}, use_global_device_ids=true, to_apply=%region_8.9 | all-reduce | flops 256 | bytes 2048 | tf_op jit(solution)/shard_map/psum | solution.py:87
  159.7 0.0 copy-done.2
  159.7 0.8 multiply_convert_fusion.1
  (5 shorter events, 0.1 us)
Async XLA Ops:
  6.5 13.2 %copy-start = (bf16[256,512]{1,0:T(8,128)(2,1)S(1)}, bf16[256,512]{1,0:T(8,128)(2,1)}, u32[]{:S(2)}) copy-start(bf16[256,512]{1,0:T(8,128)(2,1)} %param.8) | copy-start | bytes 786436
  6.5 13.2 %copy-start.1 = (f32[512]{0:T(512)S(1)}, f32[512]{0:T(512)}, u32[]{:S(2)}) copy-start(f32[512]{0:T(512)} %param.11) | copy-start | bytes 6148
  6.5 60.3 %all-gather.2.cloned.1.call-start = ((), (), s32[]{:S(2)}) async-start(), calls=%async_computation.2 | async-start | bytes 3276800 | tf_op jit(solution)/shard_map/all_gather | solution.py:66
  66.9 5.6 %copy-start.3 = (bf16[1,2048,1024]{2,1,0:T(8,128)(2,1)S(1)}, bf16[1,2048,1024]{2,1,0:T(8,128)(2,1)}, u32[]{:S(2)}) copy-start(bf16[1,2048,1024]{2,1,0:T(8,128)(2,1)} %param.14) | copy-start | bytes 12582916
  66.9 5.6 %copy-start.5 = (bf16[1,640,2048]{2,1,0:T(8,128)(2,1)S(1)}, bf16[1,640,2048]{2,1,0:T(8,128)(2,1)}, u32[]{:S(2)}) copy-start(bf16[1,640,2048]{2,1,0:T(8,128)(2,1)} %all-gather.2.cloned.1.call-done) | copy-start | bytes 7864324
  75.6 30.5 %collective-permute-start.1 = (bf16[1,640,1024]{2,1,0:T(8,128)(2,1)S(1)}, bf16[1,640,1024]{2,1,0:T(8,128)(2,1)S(1)}, u32[]{:S(2)}, u32[]{:S(2)}) collective-permute-start(bf16[1,640,1024]{2,1,0:T(8,128)(2,1)S(1)} %bitcast.72), channel_id=1, source_target_pairs={{0,1},{1,2},{2,3},{3,0},{4,5},{5,6},{6,7},{7,4},{8,9},{9,10},{10,1... | collective-permute-start | bytes 3932168 | tf_op jit(solution)/shard_map/ppermute | solution.py:27
  75.9 32.4 %collective-permute-start = (bf16[1,640,1024]{2,1,0:T(8,128)(2,1)S(1)}, bf16[1,640,1024]{2,1,0:T(8,128)(2,1)}, u32[]{:S(2)}, u32[]{:S(2)}) collective-permute-start(bf16[1,640,1024]{2,1,0:T(8,128)(2,1)S(1)} %bitcast.73), channel_id=1, source_target_pairs={{0,3},{1,0},{2,1},{3,2},{4,7},{5,4},{6,5},{7,6},{8,11},{9,8},{10,9... | collective-permute-start | bytes 3932168 | tf_op jit(solution)/shard_map/ppermute | solution.py:29
  106.1 17.1 %collective-permute-start.2 = (bf16[1,640,1024]{2,1,0:T(8,128)(2,1)S(1)}, bf16[1,640,1024]{2,1,0:T(8,128)(2,1)}, u32[]{:S(2)}, u32[]{:S(2)}) collective-permute-start(bf16[1,640,1024]{2,1,0:T(8,128)(2,1)S(1)} %collective-permute-done.1), channel_id=1, source_target_pairs={{0,1},{1,2},{2,3},{3,0},{4,5},{5,6},{6,7},{7,4},{8,9},{9,10},{10,1... | collective-permute-start | bytes 3932168 | tf_op jit(solution)/shard_map/ppermute | solution.py:27
  106.1 2.5 %copy-start.4 = (bf16[1,4096,512]{2,1,0:T(8,128)(2,1)S(1)}, bf16[1,4096,512]{2,1,0:T(8,128)(2,1)}, u32[]{:S(2)}) copy-start(bf16[1,4096,512]{2,1,0:T(8,128)(2,1)} %param.15) | copy-start | bytes 12582916
  152.3 0.7 copy-start.6
  153.0 6.7 %copy-start.2 = (f32[512]{0:T(512)S(1)}, f32[512]{0:T(512)}, u32[]{:S(2)}) copy-start(f32[512]{0:T(512)} %param.12) | copy-start | bytes 6148
Sparse Core Ops, SparseCore 0:
  42.6 24.2 all-gather.1
